TPU v7x, 32 devices: a whole 2x2x4 slice. The times are simulated.
32 devices in a mesh: grp: 2 (over y), sp: 4 (over z), tp: 4 (over x, core).
Axes of the slice: x: 2, y: 2, z: 4, core: 2. Of those that a mesh axis runs over, the one named last changes fastest.
Arguments:
- queries: bfloat16 [2048, 2048], P(('grp', 'sp'), 'tp'), parts along dimension 0, may hold values from -6 to 6
- keys: bfloat16 [2048, 512], P(('grp', 'sp'), 'tp'), parts along dimension 0, may hold values from -6 to 6
- values: bfloat16 [2048, 512], P(('grp', 'sp'), 'tp'), parts along dimension 0, may hold values from -6 to 6
- query_gain: float32 [128], replicated, may hold values from 1 to 5, as said below
- key_norm_gain: float32 [128], replicated, may hold values from 1 to 5, as said below
- out_weight: bfloat16 [2048, 2048], P('tp'), may hold values from -0.125 to 0.125
- residual: bfloat16 [2048, 2048], P(('grp', 'sp')), parts along dimension 0, may hold values from -0.59765625 to 0.59765625
- mixer_gain: float32 [2048], replicated, may hold values from 0.1 to 1.9
- gate_weight: bfloat16 [2048, 5632], P('sp', 'tp'), may hold values from -0.125 to 0.125
- up_weight: bfloat16 [2048, 5632], P('sp', 'tp'), may hold values from -0.125 to 0.125
- conv_taps: float32 [3, 5632], P(None, 'tp'), may hold values from -3.5 to 3.5
- down_weight: bfloat16 [5632, 2048], P('tp', 'sp'), may hold values from -0.078125 to 0.078125
Outputs:
- layer_out: bfloat16 [2048, 2048], P(('grp', 'sp', 'tp')), parts along dimension 0
There are 2 independent parts, one for each index of `grp`. A program takes and returns all parts, laid end to end along the dimension named above; an argument that names none is the same for every part. Nothing has to cross between parts.
Inputs may be any that keep to these rules, and one draw needn't show every extreme that they name: `query_gain`: positive. `key_norm_gain`: positive.
All inputs are finite; a program needn't handle non-finite values.
Results may differ from a plain program's by a relative error of at most 0.024.
Values may be sent and summed in bfloat16 or wider, within the bound.
A program may use at most 128 MiB of HBM per device.

v0:
```python
import math
import jax
import jax.numpy as jnp
from jax import lax
from jax.sharding import PartitionSpec as P

GRID = 64
norm_eps = 1e-06
rope_base = 10000.0


def padded_2(block, sides, width):
    for axis, dim in sides:
        count = lax.axis_size(axis)
        forward = [(i, i + 1) for i in range(count - 1)]
        backward = [(target, source) for source, target in forward]
        low = lax.ppermute(
            lax.slice_in_dim(block, block.shape[dim] - width, None, axis=dim), axis, forward
        )
        high = lax.ppermute(lax.slice_in_dim(block, 0, width, axis=dim), axis, backward)
        block = jnp.concatenate([low, block, high], axis=dim)
    return block


def angle_tables(positions, head_dim):
    quarter = head_dim // 4
    freqs = 1.0 / rope_base ** (jnp.arange(quarter, dtype=jnp.float32) * 4.0 / head_dim)
    grid_row = (positions // GRID).astype(jnp.float32)
    grid_col = (positions % GRID).astype(jnp.float32)
    by_row = grid_row[:, None] * freqs[None, :]
    by_col = grid_col[:, None] * freqs[None, :]
    angles = jnp.concatenate([by_row, by_row, by_col, by_col], axis=-1)
    return (jnp.cos(angles), jnp.sin(angles))


def apply_rotary(field, cosine_table, sine_table):
    half = field.shape[-1] // 2
    quarter = half // 2
    first = field[..., :half]
    second = field[..., half:]
    turned = jnp.concatenate(
        [
            -first[..., quarter:],
            first[..., :quarter],
            -second[..., quarter:],
            second[..., :quarter],
        ],
        axis=-1,
    )
    return field * cosine_table[:, None, :] + turned * sine_table[:, None, :]


def per_head_norm(field, gain):
    floats = field.astype(jnp.float32)
    return floats * lax.rsqrt(jnp.mean(floats * floats, axis=-1, keepdims=True) + norm_eps) * gain


def local(
    queries,
    keys,
    values,
    query_gain,
    key_norm_gain,
    out_weight,
    residual,
    mixer_gain,
    gate_weight,
    up_weight,
    conv_taps,
    down_weight,
):
    tok_rows = queries.shape[0]
    head_dim = query_gain.shape[0]
    heads_here = queries.shape[1] // head_dim
    kv_here = keys.shape[1] // head_dim
    query_group = heads_here // kv_here
    part_rows = tok_rows // lax.axis_size("tp")
    positions = lax.axis_index("sp") * tok_rows + jnp.arange(tok_rows, dtype=jnp.int32)
    cosine_table, sine_table = angle_tables(positions, head_dim)
    rotated_queries = apply_rotary(
        per_head_norm(queries.reshape(tok_rows, heads_here, head_dim), query_gain),
        cosine_table,
        sine_table,
    ).astype(jnp.bfloat16)
    rotated_keys = apply_rotary(
        per_head_norm(keys.reshape(tok_rows, kv_here, head_dim), key_norm_gain),
        cosine_table,
        sine_table,
    ).astype(jnp.bfloat16)
    key_flat = rotated_keys.reshape(tok_rows, kv_here * head_dim)
    query_mat = jnp.transpose(
        rotated_queries.reshape(tok_rows, kv_here, query_group, head_dim), (1, 2, 0, 3)
    )
    query_mat = query_mat.reshape(kv_here, query_group * tok_rows, head_dim)
    scale = head_dim ** (-0.5)
    start_state = (
        jnp.full((kv_here, query_group * tok_rows), -jnp.inf, jnp.float32),
        jnp.zeros((kv_here, query_group * tok_rows), jnp.float32),
        jnp.zeros((kv_here, query_group * tok_rows, head_dim), jnp.float32),
    )
    key_piece = lax.all_gather(key_flat, "sp", axis=0, tiled=True)
    value_piece = lax.all_gather(values, "sp", axis=0, tiled=True)
    piece_rows = key_piece.shape[0]
    block_slice = math.gcd(piece_rows, 512)
    key_blocks = key_piece.reshape(piece_rows // block_slice, block_slice, kv_here, head_dim)
    value_blocks = value_piece.reshape(piece_rows // block_slice, block_slice, kv_here, head_dim)

    def one_block(state, block_pair):
        running, totals, accum = state
        key_block, value_block = block_pair
        scores = (
            jnp.einsum("hqd,khd->hqk", query_mat, key_block, preferred_element_type=jnp.float32)
            * scale
        )
        new_max = jnp.maximum(running, jnp.max(scores, axis=-1))
        factor = jnp.exp(running - new_max)
        expo = jnp.exp(scores - new_max[..., None])
        totals = totals * factor + jnp.sum(expo, axis=-1)
        accum = accum * factor[..., None] + jnp.einsum(
            "hqk,khd->hqd",
            expo.astype(jnp.bfloat16),
            value_block,
            preferred_element_type=jnp.float32,
        )
        return ((new_max, totals, accum), None)

    result, unused = lax.scan(one_block, start_state, (key_blocks, value_blocks))
    running, totals, accum = result
    heads = (accum / totals[..., None]).astype(jnp.bfloat16)
    heads = jnp.transpose(heads.reshape(kv_here, query_group, tok_rows, head_dim), (2, 0, 1, 3))
    heads = heads.reshape(tok_rows, heads_here * head_dim)
    own_start = lax.axis_index("tp") * part_rows
    full_proj = lax.psum(
        jnp.dot(heads, out_weight, preferred_element_type=jnp.float32).astype(jnp.bfloat16), "tp"
    ).astype(jnp.float32)
    mixed = residual.astype(jnp.float32) + full_proj
    normed = per_head_norm(mixed, mixer_gain).astype(jnp.bfloat16)
    mixed_keep = lax.dynamic_slice_in_dim(mixed, own_start, part_rows, 0)
    gate_acc = jnp.dot(
        normed,
        lax.all_gather(gate_weight, "sp", axis=0, tiled=True),
        preferred_element_type=jnp.float32,
    )
    up_acc = jnp.dot(
        normed,
        lax.all_gather(up_weight, "sp", axis=0, tiled=True),
        preferred_element_type=jnp.float32,
    )
    gate = gate_acc.astype(jnp.bfloat16)
    up_val = up_acc.astype(jnp.bfloat16)
    padded = padded_2(gate, (("sp", 0),), 1).astype(jnp.float32)
    conv = conv_taps[0] * padded[:-2] + conv_taps[1] * padded[1:-1] + conv_taps[2] * padded[2:]
    hidden = (jax.nn.silu(conv) * up_val.astype(jnp.float32)).astype(jnp.bfloat16)
    down_full = lax.all_gather(down_weight, "sp", axis=1, tiled=True)
    mixer_out = lax.psum_scatter(
        jnp.dot(hidden, down_full, preferred_element_type=jnp.float32).astype(jnp.bfloat16),
        "tp",
        scatter_dimension=0,
        tiled=True,
    ).astype(jnp.float32)
    return (mixed_keep + mixer_out).astype(jnp.bfloat16)


def solution(mesh):
    in_specs = (
        P(("grp", "sp"), "tp"),
        P(("grp", "sp"), "tp"),
        P(("grp", "sp"), "tp"),
        P(),
        P(),
        P("tp", None),
        P(("grp", "sp"), None),
        P(),
        P("sp", "tp"),
        P("sp", "tp"),
        P(None, "tp"),
        P("tp", "sp"),
    )
    out_specs = P(("grp", "sp", "tp"), None)
    return jax.shard_map(local, mesh=mesh, in_specs=in_specs, out_specs=out_specs, check_vma=False)
```

profile of v0, /device:TPU:0, one launch (start us, length us, event | category | flops | bytes accessed | tf_op | source)
XLA Modules:
  0.0 424.0 jit_solution(16997622798966750573)
XLA Ops:
  7.4 1.3 reshape.324
  8.7 1.9 reshape.323
  15.2 1.2 fusion.31
  16.4 15.7 %all_gather.15 = bf16[1024,128]{1,0:T(8,128)(2,1)S(1)} all-gather(bf16[256,128]{1,0:T(8,128)(2,1)S(1)} %get-tuple-element.109), channel_id=1, replica_groups=mesh['grp'=2,'sp'=4,'tp'=4] {'sp'}, dimensions={0}, use_global_device_ids=true | all-gather | bytes 327680 | tf_op jit(solution)/shard_map/all_gather | solution.py:101
  32.0 14.6 %all_gather.16 = bf16[1024,128]{1,0:T(8,128)(2,1)S(1)} all-gather(bf16[256,128]{1,0:T(8,128)(2,1)S(1)} %copy-done.4), channel_id=1, replica_groups=mesh['grp'=2,'sp'=4,'tp'=4] {'sp'}, dimensions={0}, use_global_device_ids=true | all-gather | bytes 327680 | tf_op jit(solution)/shard_map/all_gather | solution.py:102
  46.6 9.3 %while.15 = (s32[]{:T(128)}, f32[1,1024]{1,0:T(1,128)S(1)}, f32[1,1024]{1,0:T(1,128)S(1)}, f32[1,1024,128]{2,1,0:T(8,128)S(1)}, bf16[2,512,1,128]{3,1,2,0:T(8,12...) while((s32[]{:T(128)}, f32[1,1024]{1,0:T(1,128)S(1)}, ...), condition=%wide.region_5.6_spmd.clone, body=%wide.region_2.5_spmd.clone.sunk | while | flops 273028096 | bytes 16318605 | solution.py:127
  46.6 1.8 multiply_reduce_fusion.4
  48.4 2.1 fusion.63
  51.3 1.8 multiply_reduce_fusion.4
  53.1 2.1 fusion.63
  56.3 1.7 convolution_convert_fusion
  59.8 35.8 %all-reduce.2.cloned.1.call-done = bf16[256,2048]{1,0:T(8,128)(2,1)} async-done(((bf16[256,2048]{1,0:T(8,128)(2,1)}), bf16[256,2048]{1,0:T(8,128)(2,1)}) %all-reduce.2.cloned.1.call-update) | async-done | bytes 1048592 | tf_op jit(solution)/shard_map/psum | solution.py:133
  95.7 3.2 convert_add_fusion
  98.9 68.7 %all-gather.4.cloned.1.call-done = bf16[2048,1408]{1,0:T(8,128)(2,1)} async-done(((bf16[512,1408]{1,0:T(8,128)(2,1)}), bf16[2048,1408]{1,0:T(8,128)(2,1)}) %all-gather.4.cloned.1.call-update) | async-done | bytes 5767184 | tf_op jit(solution)/shard_map/all_gather | solution.py:141
  167.6 5.1 %convolution_convert_fusion.2 = bf16[256,1408]{1,0:T(8,128)(2,1)S(1)} fusion(bf16[2048,1408]{1,0:T(8,128)(2,1)} %all-gather.4.cloned.1.call-done, f32[2048]{0:T(1024)S(1)} %copy-done.8, f32[256]{0:T(256)S(1)} %add_rsqrt_fusion.1, bf16[256,2048]{1,0:T(8,128)(2,1)} %all-reduce.2.cloned.1.call-done, bf16[256,2048]{1,0:T(8,128)(2,1)} %param.20), kind=kOutput, calls=%fused_computation.29 | convolution fusion | flops 1479901184 | bytes 8594432 | tf_op jit(solution)/shard_map/dot_general | solution.py:139
  172.8 1.3 collective-permute-start
  174.1 1.5 collective-permute-start.1
  175.6 4.0 collective-permute-done.1
  179.6 1.3 maximum_convert_fusion
  180.9 93.1 %all-gather.6.cloned.1.call-done = bf16[2048,1408]{1,0:T(8,128)(2,1)} async-done(((bf16[512,1408]{1,0:T(8,128)(2,1)}), bf16[2048,1408]{1,0:T(8,128)(2,1)}) %all-gather.6.cloned.1.call-update) | async-done | bytes 5767184 | tf_op jit(solution)/shard_map/all_gather | solution.py:146
  274.0 106.2 %all-gather.8.cloned.1.call-done = bf16[1408,2048]{1,0:T(8,128)(2,1)} async-done(((bf16[1408,512]{1,0:T(8,128)(2,1)}), bf16[1408,2048]{1,0:T(8,128)(2,1)}) %all-gather.8.cloned.1.call-update) | async-done | bytes 5767184 | tf_op jit(solution)/shard_map/all_gather | solution.py:154
  380.2 11.1 %convolution_convert_fusion.3 = bf16[256,2048]{1,0:T(8,128)(2,1)} fusion(bf16[1408,2048]{1,0:T(8,128)(2,1)} %all-gather.8.cloned.1.call-done, bf16[2048,1408]{1,0:T(8,128)(2,1)} %all-gather.6.cloned.1.call-done, f32[258,1408]{1,0:T(8,128)} %maximum_convert_fusion, f32[1408]{0:T(1024)S(1)} %get-tuple-element.91, f32[1408]{0:T(1024)S(1)} %get-tuple-element.92, ...), kind=kOutput, calls=%fused_computation.30 | convolution fusion | flops 2961145856 | bytes 19031552 | tf_op jit(solution)/shard_map/dot_general | solution.py:156
  391.3 23.2 %reduce-scatter.2.cloned.1.call-done = bf16[64,2048]{1,0:T(8,128)(2,1)} async-done(((bf16[256,2048]{1,0:T(8,128)(2,1)}), bf16[64,2048]{1,0:T(8,128)(2,1)}) %reduce-scatter.2.cloned.1.call-update) | async-done | bytes 262160 | tf_op jit(solution)/shard_map/reduce_scatter | solution.py:155
  414.5 1.9 add_convert_fusion
  (60 shorter events, 8.2 us)
Async XLA Ops:
  7.4 48.9 %copy-start = (bf16[512,2048]{1,0:T(8,128)(2,1)S(1)}, bf16[512,2048]{1,0:T(8,128)(2,1)}, u32[]{:S(2)}) copy-start(bf16[512,2048]{1,0:T(8,128)(2,1)} %param.19) | copy-start | bytes 6291460
  7.4 5.7 %copy-start.7 = (f32[128]{0:T(128)S(1)}, f32[128]{0:T(128)}, u32[]{:S(2)}) copy-start(f32[128]{0:T(128)} %param.17) | copy-start | bytes 1540
  7.4 88.3 %all-reduce.2.cloned.1.call-start = ((), (), s32[]{:S(2)}) async-start(), calls=%async_computation.1 | async-start | bytes 2097152 | tf_op jit(solution)/shard_map/psum | solution.py:133
  13.4 1.1 copy-start.3
  13.4 1.1 copy-start.6
  13.4 1.7 copy-start.2
  15.1 16.9 %copy-start.4 = (bf16[256,128]{1,0:T(8,128)(2,1)S(1)}, bf16[256,128]{1,0:T(8,128)(2,1)}, u32[]{:S(2)}) copy-start(bf16[256,128]{1,0:T(8,128)(2,1)} %param.16) | copy-start | bytes 196612
  48.4 2.2 copy-start.1
  53.0 2.2 copy-start.1
  58.0 109.6 %all-gather.4.cloned.1.call-start = ((), (), s32[]{:S(2)}) async-start(), calls=%async_computation.2 | async-start | bytes 7208960 | tf_op jit(solution)/shard_map/all_gather | solution.py:141
  58.6 215.4 %all-gather.6.cloned.1.call-start = ((), (), s32[]{:S(2)}) async-start(), calls=%async_computation.3 | async-start | bytes 7208960 | tf_op jit(solution)/shard_map/all_gather | solution.py:146
  59.2 321.0 %all-gather.8.cloned.1.call-start = ((), (), s32[]{:S(2)}) async-start(), calls=%async_computation.4 | async-start | bytes 7208960 | tf_op jit(solution)/shard_map/all_gather | solution.py:154
  59.8 107.8 %copy-start.8 = (f32[2048]{0:T(1024)S(1)}, f32[2048]{0:T(1024)}, u32[]{:S(2)}) copy-start(f32[2048]{0:T(1024)} %param.21) | copy-start | bytes 24580
  59.8 354.7 %reduce-scatter.2.cloned.1.call-start = ((), (), s32[]{:S(2)}) async-start(), calls=%async_computation.5 | async-start | bytes 1310720 | tf_op jit(solution)/shard_map/reduce_scatter | solution.py:155
  98.9 76.6 %copy-start.5 = (f32[3,1408]{1,0:T(4,128)S(1)}, f32[3,1408]{1,0:T(4,128)}, u32[]{:S(2)}) copy-start(f32[3,1408]{1,0:T(4,128)} %param.24) | copy-start | bytes 50692
  172.8 2.8 collective-permute-start
  174.1 5.5 %collective-permute-start.1 = (bf16[1,1408]{1,0:T(2,128)(2,1)S(1)}, bf16[1,1408]{1,0:T(2,128)(2,1)S(1)}, u32[]{:S(2)}, u32[]{:S(2)}) collective-permute-start(bf16[1,1408]{1,0:T(2,128)(2,1)S(1)} %get-tuple-element.117), channel_id=1, source_target_pairs={{4,0},{8,4},{12,8},{5,1},{9,5},{13,9},{6,2},{10,6},{14,10},{7,3},{... | collective-permute-start | bytes 8456 | tf_op jit(solution)/shard_map/ppermute | solution.py:20
Sparse Core Ops, SparseCore 0:
  58.1 37.4 all-reduce.1
  391.4 23.0 reduce-scatter.1
Sparse Core Ops, SparseCore 1:
  60.1 107.5 all-gather.3
  169.0 104.9 all-gather.5
  275.4 104.7 all-gather.7
where the time goes:
time: 424 us
  waiting for transfers between devices  333 us (79%)
  blocking collectives  30.2 us (7%)
  matrix products  22.8 us (5%)
  other arithmetic  16.5 us (4%)
  between operations  15.3 us (4%)
    all_gather x1, waiting for transfers between devices, local(): down_full = lax.all_gather(down_weight, 'sp', axis=1, tiled=True)  106 us
    all_gather x1, waiting for transfers between devices, local(): lax.all_gather(up_weight, 'sp', axis=0, tiled=True)  93.1 us
    all_gather x1, waiting for transfers between devices, local(): lax.all_gather(gate_weight, 'sp', axis=0, tiled=True)  68.7 us
    psum x1, waiting for transfers between devices, local(): lax.psum(jnp.dot(heads, out_weight, preferred_element_type=jnp.float32).a...  35.8 us
    reduce_scatter x1, waiting for transfers between devices, local(): lax.psum_scatter(jnp.dot(hidden, down_full, preferred_element_type=jnp.fl...  23.2 us
    all_gather x1, blocking collectives, local(): key_piece = lax.all_gather(key_flat, 'sp', axis=0, tiled=True)  15.7 us
    all_gather x1, blocking collectives, local(): value_piece = lax.all_gather(values, 'sp', axis=0, tiled=True)  14.6 us
    dot_general x1, matrix products, local(): jnp.dot(hidden, down_full, preferred_element_type=jnp.float32)  11.1 us
  transfers between devices with their start and end apart: 7, of which 6 were waited for; matrix products, arithmetic and copies ran while one was open for 2% of the time, Pallas kernels for 0%

commit v1 on v0

--- a/solution.py
+++ b/solution.py
@@ -130,8 +130,12 @@
     heads = jnp.transpose(heads.reshape(kv_here, query_group, tok_rows, head_dim), (2, 0, 1, 3))
     heads = heads.reshape(tok_rows, heads_here * head_dim)
     own_start = lax.axis_index("tp") * part_rows
-    full_proj = lax.psum(
-        jnp.dot(heads, out_weight, preferred_element_type=jnp.float32).astype(jnp.bfloat16), "tp"
+    full_proj = jnp.sum(
+        lax.all_gather(
+            jnp.dot(heads, out_weight, preferred_element_type=jnp.float32).astype(jnp.bfloat16),
+            "tp",
+        ),
+        axis=0,
     ).astype(jnp.float32)
     mixed = residual.astype(jnp.float32) + full_proj
     normed = per_head_norm(mixed, mixer_gain).astype(jnp.bfloat16)

time: 424 us -> 457 us (1.078)
  waiting for transfers between devices: 333 us -> 363 us
    psum x1 -> x0, waiting for transfers between devices: 35.8 us -> none  [local(): lax.psum(jnp.dot(heads, out_weight, preferred_element_type=jnp.float32).a...]
    all_gather x0 -> x1, waiting for transfers between devices: none -> 33.4 us  [local(): lax.all_gather(jnp.dot(heads, out_weight, preferred_element_type=jnp.floa...]
    all_gather x1, waiting for transfers between devices: 68.7 us -> 101 us  [local(): lax.all_gather(gate_weight, 'sp', axis=0, tiled=True)]
    all_gather x1, waiting for transfers between devices: 93.1 us -> 106 us  [local(): lax.all_gather(up_weight, 'sp', axis=0, tiled=True)]
    all_gather x1, waiting for transfers between devices: 106 us -> 93.3 us  [local(): down_full = lax.all_gather(down_weight, 'sp', axis=1, tiled=True)]
  transfers between devices with their start and end apart: 7 -> 7, of which waited for: 6 -> 6; matrix products, arithmetic and copies ran while one was open for 2% -> 3% of each run, Pallas kernels for 0% -> 0%
where the time goes in v1:
time: 457 us
  waiting for transfers between devices  363 us (79%)
  blocking collectives  30.2 us (7%)
  matrix products  22.8 us (5%)
  other arithmetic  20.8 us (5%)
  between operations  13.4 us (3%)
    all_gather x1, waiting for transfers between devices, local(): lax.all_gather(up_weight, 'sp', axis=0, tiled=True)  106 us
    all_gather x1, waiting for transfers between devices, local(): lax.all_gather(gate_weight, 'sp', axis=0, tiled=True)  101 us
    all_gather x1, waiting for transfers between devices, local(): down_full = lax.all_gather(down_weight, 'sp', axis=1, tiled=True)  93.3 us
    all_gather x1, waiting for transfers between devices, local(): lax.all_gather(jnp.dot(heads, out_weight, preferred_element_type=jnp.floa...  33.4 us
    reduce_scatter x1, waiting for transfers between devices, local(): lax.psum_scatter(jnp.dot(hidden, down_full, preferred_element_type=jnp.fl...  23.2 us
    all_gather x1, blocking collectives, local(): key_piece = lax.all_gather(key_flat, 'sp', axis=0, tiled=True)  15.7 us
    all_gather x1, blocking collectives, local(): value_piece = lax.all_gather(values, 'sp', axis=0, tiled=True)  14.6 us
    dot_general x1, matrix products, local(): jnp.dot(hidden, down_full, preferred_element_type=jnp.float32)  11 us
  transfers between devices with their start and end apart: 7, of which 6 were waited for; matrix products, arithmetic and copies ran while one was open for 3% of the time, Pallas kernels for 0%

profile of v1, /device:TPU:0, one launch (start us, length us, event | category | flops | bytes accessed | tf_op | source)
XLA Modules:
  0.0 456.7 jit_solution(18411397507224111477)
XLA Ops:
  6.6 1.3 reshape.324
  7.8 1.9 reshape.323
  15.5 15.7 %all_gather.21 = bf16[1024,128]{1,0:T(8,128)(2,1)S(1)} all-gather(bf16[256,128]{1,0:T(8,128)(2,1)S(1)} %get-tuple-element.109), channel_id=1, replica_groups=mesh['grp'=2,'sp'=4,'tp'=4] {'sp'}, dimensions={0}, use_global_device_ids=true | all-gather | bytes 327680 | tf_op jit(solution)/shard_map/all_gather | solution.py:101
  31.2 14.6 %all_gather.22 = bf16[1024,128]{1,0:T(8,128)(2,1)S(1)} all-gather(bf16[256,128]{1,0:T(8,128)(2,1)S(1)} %copy-done.4), channel_id=1, replica_groups=mesh['grp'=2,'sp'=4,'tp'=4] {'sp'}, dimensions={0}, use_global_device_ids=true | all-gather | bytes 327680 | tf_op jit(solution)/shard_map/all_gather | solution.py:102
  45.8 9.3 %while.15 = (s32[]{:T(128)}, f32[1,1024]{1,0:T(1,128)S(1)}, f32[1,1024]{1,0:T(1,128)S(1)}, f32[1,1024,128]{2,1,0:T(8,128)S(1)}, bf16[2,512,1,128]{3,1,2,0:T(8,12...) while((s32[]{:T(128)}, f32[1,1024]{1,0:T(1,128)S(1)}, ...), condition=%wide.region_5.6_spmd.clone, body=%wide.region_2.5_spmd.clone.sunk | while | flops 273028096 | bytes 16318605 | solution.py:127
  45.8 1.8 multiply_reduce_fusion.4
  47.6 2.1 fusion.63
  50.4 1.8 multiply_reduce_fusion.4
  52.2 2.1 fusion.63
  55.5 1.7 convolution_convert_fusion
  59.3 33.4 %all-gather.12.cloned.1.call-done = bf16[1024,2048]{1,0:T(8,128)(2,1)} async-done(((bf16[256,2048]{1,0:T(8,128)(2,1)}), bf16[1024,2048]{1,0:T(8,128)(2,1)}) %all-gather.12.cloned.1.call-update) | async-done | bytes 4194320 | tf_op jit(solution)/shard_map/all_gather | solution.py:134
  92.8 4.3 reduce_sum.52
  97.1 3.2 convert_add_fusion
  100.3 100.7 %all-gather.6.cloned.1.call-done = bf16[2048,1408]{1,0:T(8,128)(2,1)} async-done(((bf16[512,1408]{1,0:T(8,128)(2,1)}), bf16[2048,1408]{1,0:T(8,128)(2,1)}) %all-gather.6.cloned.1.call-update) | async-done | bytes 5767184 | tf_op jit(solution)/shard_map/all_gather | solution.py:145
  201.1 5.2 %convolution_convert_fusion.2 = bf16[256,1408]{1,0:T(8,128)(2,1)S(1)} fusion(bf16[2048,1408]{1,0:T(8,128)(2,1)} %all-gather.6.cloned.1.call-done, f32[2048]{0:T(1024)S(1)} %copy-done.8, f32[256]{0:T(256)S(1)} %add_rsqrt_fusion.1, bf16[256,2048]{1,0:T(8,128)(2,1)} %reduce_sum.52, bf16[256,2048]{1,0:T(8,128)(2,1)} %param.20), kind=kOutput, calls=%fused_computation.29 | convolution fusion | flops 1479901184 | bytes 8594432 | tf_op jit(solution)/shard_map/dot_general | solution.py:143
  206.3 1.3 collective-permute-start
  207.6 1.5 collective-permute-start.1
  209.1 4.0 collective-permute-done.1
  213.1 1.3 maximum_convert_fusion
  214.4 93.3 %all-gather.10.cloned.1.call-done = bf16[1408,2048]{1,0:T(8,128)(2,1)} async-done(((bf16[1408,512]{1,0:T(8,128)(2,1)}), bf16[1408,2048]{1,0:T(8,128)(2,1)}) %all-gather.10.cloned.1.call-update) | async-done | bytes 5767184 | tf_op jit(solution)/shard_map/all_gather | solution.py:158
  307.7 106.4 %all-gather.8.cloned.1.call-done = bf16[2048,1408]{1,0:T(8,128)(2,1)} async-done(((bf16[512,1408]{1,0:T(8,128)(2,1)}), bf16[2048,1408]{1,0:T(8,128)(2,1)}) %all-gather.8.cloned.1.call-update) | async-done | bytes 5767184 | tf_op jit(solution)/shard_map/all_gather | solution.py:150
  414.0 11.0 %convolution_convert_fusion.3 = bf16[256,2048]{1,0:T(8,128)(2,1)} fusion(bf16[1408,2048]{1,0:T(8,128)(2,1)} %all-gather.10.cloned.1.call-done, bf16[2048,1408]{1,0:T(8,128)(2,1)} %all-gather.8.cloned.1.call-done, f32[258,1408]{1,0:T(8,128)} %maximum_convert_fusion, f32[1408]{0:T(1024)S(1)} %get-tuple-element.91, f32[1408]{0:T(1024)S(1)} %get-tuple-element.92, ...), kind=kOutput, calls=%fused_computation.30 | convolution fusion | flops 2961145856 | bytes 19031552 | tf_op jit(solution)/shard_map/dot_general | solution.py:160
  425.1 23.2 %reduce-scatter.2.cloned.1.call-done = bf16[64,2048]{1,0:T(8,128)(2,1)} async-done(((bf16[256,2048]{1,0:T(8,128)(2,1)}), bf16[64,2048]{1,0:T(8,128)(2,1)}) %reduce-scatter.2.cloned.1.call-update) | async-done | bytes 262160 | tf_op jit(solution)/shard_map/reduce_scatter | solution.py:159
  448.3 1.9 add_convert_fusion
  (61 shorter events, 9.7 us)
Async XLA Ops:
  6.5 48.9 %copy-start = (bf16[512,2048]{1,0:T(8,128)(2,1)S(1)}, bf16[512,2048]{1,0:T(8,128)(2,1)}, u32[]{:S(2)}) copy-start(bf16[512,2048]{1,0:T(8,128)(2,1)} %param.19) | copy-start | bytes 6291460
  6.5 5.7 %copy-start.7 = (f32[128]{0:T(128)S(1)}, f32[128]{0:T(128)}, u32[]{:S(2)}) copy-start(f32[128]{0:T(128)} %param.17) | copy-start | bytes 1540
  6.5 86.2 %all-gather.12.cloned.1.call-start = ((), (), s32[]{:S(2)}) async-start(), calls=%async_computation.5 | async-start | bytes 5242880 | tf_op jit(solution)/shard_map/all_gather | solution.py:134
  12.6 1.1 copy-start.3
  12.6 1.1 copy-start.6
  12.6 1.7 copy-start.2
  14.3 16.9 %copy-start.4 = (bf16[256,128]{1,0:T(8,128)(2,1)S(1)}, bf16[256,128]{1,0:T(8,128)(2,1)}, u32[]{:S(2)}) copy-start(bf16[256,128]{1,0:T(8,128)(2,1)} %param.16) | copy-start | bytes 196612
  47.5 2.2 copy-start.1
  52.2 2.2 copy-start.1
  57.2 143.8 %all-gather.6.cloned.1.call-start = ((), (), s32[]{:S(2)}) async-start(), calls=%async_computation.1 | async-start | bytes 7208960 | tf_op jit(solution)/shard_map/all_gather | solution.py:145
  58.0 249.7 %all-gather.10.cloned.1.call-start = ((), (), s32[]{:S(2)}) async-start(), calls=%async_computation.3 | async-start | bytes 7208960 | tf_op jit(solution)/shard_map/all_gather | solution.py:158
  58.7 355.3 %all-gather.8.cloned.1.call-start = ((), (), s32[]{:S(2)}) async-start(), calls=%async_computation.2 | async-start | bytes 7208960 | tf_op jit(solution)/shard_map/all_gather | solution.py:150
  59.3 389.0 %reduce-scatter.2.cloned.1.call-start = ((), (), s32[]{:S(2)}) async-start(), calls=%async_computation.4 | async-start | bytes 1310720 | tf_op jit(solution)/shard_map/reduce_scatter | solution.py:159
  97.1 104.0 %copy-start.8 = (f32[2048]{0:T(1024)S(1)}, f32[2048]{0:T(1024)}, u32[]{:S(2)}) copy-start(f32[2048]{0:T(1024)} %param.21) | copy-start | bytes 24580
  100.3 108.7 %copy-start.5 = (f32[3,1408]{1,0:T(4,128)S(1)}, f32[3,1408]{1,0:T(4,128)}, u32[]{:S(2)}) copy-start(f32[3,1408]{1,0:T(4,128)} %param.24) | copy-start | bytes 50692
  206.3 2.8 collective-permute-start
  207.6 5.5 %collective-permute-start.1 = (bf16[1,1408]{1,0:T(2,128)(2,1)S(1)}, bf16[1,1408]{1,0:T(2,128)(2,1)S(1)}, u32[]{:S(2)}, u32[]{:S(2)}) collective-permute-start(bf16[1,1408]{1,0:T(2,128)(2,1)S(1)} %get-tuple-element.117), channel_id=1, source_target_pairs={{4,0},{8,4},{12,8},{5,1},{9,5},{13,9},{6,2},{10,6},{14,10},{7,3},{... | collective-permute-start | bytes 8456 | tf_op jit(solution)/shard_map/ppermute | solution.py:20
Sparse Core Ops, SparseCore 0:
  57.4 35.3 all-gather.11
  94.4 106.6 all-gather.5
  202.7 104.9 all-gather.9
  309.1 104.8 all-gather.7
  425.2 23.0 reduce-scatter.1
